TPU v7x, 32 devices: a whole 2x2x4 slice. The times are simulated.
32 devices in a mesh: fs: 4 (over z), tp: 8 (over y, x, core).
Axes of the slice: x: 2, y: 2, z: 4, core: 2. Of those that a mesh axis runs over, the one named last changes fastest.
Arguments:
- tokens: bfloat16 [1024, 2048], P('fs', 'tp'), may hold values from -6 to 6
- norm_gain: float32 [2048], P('tp'), may hold values from 0.1 to 1.9
- gate_master: float32 [8, 3584, 2048], P(None, 'fs', 'tp'), may hold values from -0.125 to 0.125
- up_master: float32 [8, 3584, 2048], P(None, 'fs', 'tp'), may hold values from -0.125 to 0.125
- down_master: float32 [8, 3584, 2048], P(None, 'fs', 'tp'), may hold values from -0.0625 to 0.0625
- routes: int32 [1024, 2], P('fs'), may hold values from 0 to 3, all different within a row; in each aligned block of 256 rows (0 to 255, 256 to 511, ...) at most 128 rows name the same one
- route_logits: float32 [1024, 2], P('fs'), may hold values from -8 to 8
Outputs:
- gate_serve: bfloat16 [8, 3584, 2048], P('tp', 'fs')
- up_serve: bfloat16 [8, 3584, 2048], P('tp', 'fs')
- down_serve: bfloat16 [8, 3584, 2048], P('tp', 'fs')
- mixed_tokens: bfloat16 [1024, 2048], P('fs', 'tp')
Inputs may be any that keep to these rules, and one draw needn't show every extreme that they name: `routes`: each row names 2 different experts; in every aligned block of 256 rows each expert is named by exactly 128 rows.
All inputs are finite; a program needn't handle non-finite values.
Results may differ from a plain program's by a relative error of at most 0.024.
Values may be sent and summed in bfloat16 or wider, within the bound.
A program may use at most 128 MiB of HBM per device.

v0:
```python
import functools

import jax
import jax.numpy as jnp
from jax import lax
from jax.experimental import pallas as pl
from jax.experimental.pallas import tpu as pltpu
from jax.sharding import PartitionSpec as P

epsilon = 1e-05
MESH = pl.DeviceIdType.MESH
NT = (((1,), (1,)), ((), ()))
NN = (((1,), (0,)), ((), ()))
TN = (((0,), (0,)), ((), ()))
SLOTS = 4


def dot(a, b, dims):
    return lax.dot_general(a, b, dims, preferred_element_type=jnp.float32)


def flipped(index, mask):
    result, bit = index, 1
    while bit <= mask:
        if mask & bit:
            result = result + bit * (1 - 2 * ((index // bit) % 2))
        bit *= 2
    return result


def kernel(
    nf, nt, tok_ref, gain_ref, gate_ref, up_ref, down_ref, routes_ref, logits_ref,
    gate_out, up_out, down_out, mixed_ref,
    stage, snd, wv, comb_hi, comb_lo, pick, xin, xall, gate_pre, hid, part, pin, psum, zin, ret,
    stage_sem, w_send, w_recv, x_send, x_recv, z_send, z_recv, p_send, p_recv,
    h_send, h_recv, s_send, s_recv, r_send, r_recv, out_sem,
):
    f, me = lax.axis_index("fs"), lax.axis_index("tp")
    parity = me % 2
    partner = me + 1 - 2 * parity
    rows, cols = tok_ref.shape
    block = gate_ref.shape[1]
    half = pick.shape[1]
    cap = 2 * half
    experts = nt // 2
    masters = (gate_ref, up_ref, down_ref)
    outs = (gate_out, up_out, down_out)
    order = list(range(nt - 1, -1, -1))
    jobs = [(w, k) for w in range(3) for k in order]
    corner = [k for k in order if (k // 2).bit_count() > 1]
    later = [k for k in order if k // 2 > 1 and k not in corner]

    def load(i):
        w, k = jobs[i]
        return pltpu.make_async_copy(
            masters[w].at[flipped(me, k)], stage.at[i % SLOTS], stage_sem.at[i % SLOTS]
        )

    def remote(src, dst, send, recv, to_f, to_t):
        return pltpu.make_async_remote_copy(
            src_ref=src, dst_ref=dst, send_sem=send, recv_sem=recv,
            device_id=(to_f, to_t), device_id_type=MESH,
        )

    for i in range(SLOTS):
        load(i).start()
    barrier = pltpu.get_barrier_semaphore()
    for k in range(1, nt):
        pl.semaphore_signal(barrier, inc=1, device_id=(f, flipped(me, k)), device_id_type=MESH)

    @pl.loop(1, nf)
    def _(d):
        pl.semaphore_signal(barrier, inc=1, device_id=((f + d) % nf, me), device_id_type=MESH)

    pl.semaphore_wait(barrier, nt - 1 + nf - 1)

    step = 128 if block % 128 == 0 else block

    def weight_copy(w, k):
        return remote(
            snd.at[w, k - 1], wv.at[w, me], w_send.at[w, k - 1], w_recv.at[w, k - 1], f, flipped(me, k)
        )

    def convert(i):
        w, k = jobs[i]
        slot = i % SLOTS
        load(i).wait()
        gain = gain_ref[...]

        @pl.loop(0, block // step)
        def _(c):
            at = pl.ds(pl.multiple_of(c * step, 16), step)
            value = stage[slot, at, :]
            if w < 2:
                value = value * gain
            value = value.astype(jnp.bfloat16)
            if k:
                snd[w, k - 1, at, :] = value
            else:
                wv[w, me, at, :] = value

        if k and k not in later:
            weight_copy(w, k).start()
        if i + SLOTS < len(jobs):
            load(i + SLOTS).start()

    def x_copy(k):
        to = flipped(me, k)
        return remote(pick.at[to], xin.at[me], x_send.at[k - 1], x_recv.at[k - 1], f, to)

    def route():
        r0, r1 = routes_ref[0:1, :], routes_ref[1:2, :]
        l0, l1 = logits_ref[0:1, :], logits_ref[1:2, :]
        p0 = 1.0 / (1.0 + jnp.exp(l1 - l0))
        p1 = 1.0 / (1.0 + jnp.exp(l0 - l1))
        padded = -(-experts // 8) * 8
        ids = lax.broadcasted_iota(jnp.int32, (padded, rows), 0)
        first = jnp.where(ids == r0, 1.0, 0.0)
        second = jnp.where(ids == r1, 1.0, 0.0)
        chosen = first + second
        weight = first * p0 + second * p1
        before = lax.broadcasted_iota(jnp.int32, (rows, rows), 0)
        after = lax.broadcasted_iota(jnp.int32, (rows, rows), 1)
        upto = jnp.where(before <= after, 1.0, 0.0).astype(jnp.bfloat16)
        position = dot(chosen.astype(jnp.bfloat16), upto, NN) - 1.0
        slots = lax.broadcasted_iota(jnp.int32, (cap, rows), 0).astype(jnp.float32)
        for e in range(experts):
            hit = jnp.where(slots == position[e : e + 1, :], 1.0, 0.0) * chosen[e : e + 1, :]
            placed = hit.astype(jnp.bfloat16)
            scaled = hit * weight[e : e + 1, :]
            high = scaled.astype(jnp.bfloat16)
            at = pl.ds(e * cap, cap)
            comb_hi[at, :] = high
            comb_lo[at, :] = (scaled - high.astype(jnp.float32)).astype(jnp.bfloat16)
            got = dot(placed, tok_ref[...], NN).astype(jnp.bfloat16)
            pick[2 * e] = got[:half]
            pick[2 * e + 1] = got[half:]
        xin[me] = pick[me]
        for k in order[:-1]:
            x_copy(k).start()

    def release(w):
        for k in corner:
            weight_copy(w, k).wait_send()
        for k in later:
            weight_copy(w, k).start()

    early = 2
    for i in range(early):
        convert(i)
    route()
    for i in range(early, len(jobs)):
        convert(i)
    release(0)

    for k in order[:-1]:
        x_copy(k).wait_recv()
    total = jnp.zeros((half, 1), jnp.float32)
    for s in range(nt):
        v = xin[s].astype(jnp.float32)
        total = total + jnp.sum(v * v, axis=-1, keepdims=True)
    scale = lax.rsqrt(total / (nt * cols) + epsilon)

    def rows_of(p, g):
        return pl.ds(pl.multiple_of((p * nf + g) * half, 16), half)

    mine = rows_of(parity, f)
    for s in range(nt):
        xall[s, mine, :] = (xin[s].astype(jnp.float32) * scale).astype(jnp.bfloat16)

    def z_copy(d):
        here = xall.at[:, mine, :]
        return remote(here, here, z_send.at[d], z_recv.at[d], (f + d) % nf, me)

    def p_copy(d):
        here = xall.at[:, rows_of(parity, (f + nf - d) % nf), :]
        return remote(here, here, p_send.at[d], p_recv.at[d], f, partner)

    p_copy(0).start()

    @pl.loop(1, nf)
    def _(d):
        z_copy(d).start()

    @pl.loop(1, nf)
    def _(d):
        here = xall.at[:, rows_of(parity, (f + nf - d) % nf), :]
        remote(here, here, z_send.at[d], z_recv.at[d], (f + d) % nf, me).wait_recv()
        p_copy(d).start()

    @pl.loop(0, nf)
    def _(d):
        here = xall.at[:, rows_of(1 - parity, (f + nf - d) % nf), :]
        remote(here, here, p_send.at[d], p_recv.at[d], f, partner).wait_recv()

    def out_copy(w, k):
        s = flipped(me, k)
        to = outs[w].at[0, :, pl.ds(pl.multiple_of(s * cols, 128), cols)]
        return pltpu.make_async_copy(wv.at[w, s], to, out_sem.at[w, k])

    def arrived(w, k):
        if k:
            s = flipped(me, k)
            remote(
                snd.at[w, k - 1], wv.at[w, s], w_send.at[w, k - 1], w_recv.at[w, k - 1], f, s
            ).wait_recv()
        out_copy(w, k).start()

    def product(w, at):
        acc = dot(xall[0], wv[w, 0, at, :], NT)
        for s in range(1, nt):
            acc = acc + dot(xall[s], wv[w, s, at, :], NT)
        return acc

    def tile(c):
        return pl.ds(pl.multiple_of(c * step, 16), step)

    def lanes(c):
        return pl.ds(pl.multiple_of(c * step, 128), step) if block % 128 == 0 else slice(None)

    for k in order:
        arrived(0, k)

    @pl.loop(0, block // step)
    def _(c):
        gate_pre[:, lanes(c)] = product(0, tile(c))

    release(1)
    for k in order:
        arrived(1, k)

    @pl.loop(0, block // step)
    def _(c):
        gate = gate_pre[:, lanes(c)]
        hid[:, lanes(c)] = (gate / (1.0 + jnp.exp(-gate)) * product(1, tile(c))).astype(jnp.bfloat16)

    release(2)

    side = nf * half
    turns = [0] + list(range(nt // 2 - 1, 0, -1))

    def pair_at(g):
        return flipped(me // 2, turns[g])

    def side_rows(p):
        return pl.ds(pl.multiple_of(p * side, 16), side)

    def h_copy(g):
        q = pair_at(g)
        return remote(
            part.at[q, :, side_rows(1 - parity), :], pin.at[q], h_send.at[g], h_recv.at[g], f, partner
        )

    def s_copy(g, d):
        q, to = pair_at(g), (f + d) % nf
        return remote(psum.at[q, to], zin.at[g, d], s_send.at[g, d], s_recv.at[g, d], to, me)

    def r_copy(k):
        s = flipped(me, k)
        return remote(
            psum.at[s // 2, f, s % 2], ret.at[pl.ds(pl.multiple_of(me * half, 16), half), :],
            r_send.at[k - 1], r_recv.at[k - 1], f, s,
        )

    def stage_a(g):
        ks = (2 * turns[g] + 1, 2 * turns[g])
        for k in ks:
            arrived(2, k)
        q = pair_at(g)
        for o in range(2):
            part[q, o] = dot(hid[...], wv[2, 2 * q + o], NN).astype(jnp.bfloat16)
        h_copy(g).start()

    def stage_b(g):
        q = pair_at(g)
        h_copy(g).wait_recv()
        for o in range(2):
            both = part[q, o, side_rows(parity), :].astype(jnp.float32) + pin[q, o].astype(jnp.float32)
            both = both.astype(jnp.bfloat16)
            for j in range(nf):
                psum[q, j, o] = both[j * half : (j + 1) * half]

        @pl.loop(1, nf)
        def _(d):
            s_copy(g, d).start()

    def stage_c(g):
        q = pair_at(g)

        @pl.loop(1, nf)
        def _(d):
            s_copy(g, d).wait_recv()

        for o in range(2):
            acc = psum[q, f, o].astype(jnp.float32)
            for d in range(1, nf):
                acc = acc + zin[g, d, o].astype(jnp.float32)
            psum[q, f, o] = acc.astype(jnp.bfloat16)
        for k in (2 * turns[g] + 1, 2 * turns[g]):
            if k:
                r_copy(k).start()
            else:
                ret[pl.ds(pl.multiple_of(me * half, 16), half), :] = psum[me // 2, f, me % 2]

    pairs = nt // 2
    for g in range(pairs):
        stage_a(g)
        stage_b(g)
        if g:
            stage_c(g - 1)
    stage_c(pairs - 1)
    for k in order[:-1]:
        r_copy(k).wait_recv()
    mixed = dot(comb_hi[...], ret[...], TN) + dot(comb_lo[...], ret[...], TN)
    mixed_ref[...] = mixed.astype(jnp.bfloat16)

    for k in order:
        for w in range(3):
            out_copy(w, k).wait()
            if k and k not in corner:
                weight_copy(w, k).wait_send()
        if k:
            x_copy(k).wait_send()
            r_copy(k).wait_send()
    p_copy(0).wait_send()

    @pl.loop(1, nf)
    def _(d):
        z_copy(d).wait_send()
        p_copy(d).wait_send()
        for g in range(pairs):
            s_copy(g, d).wait_send()

    for g in range(pairs):
        h_copy(g).wait_send()


def local(tokens, norm_gain, gate_master, up_master, down_master, routes, route_logits):
    nf, nt = lax.axis_size("fs"), lax.axis_size("tp")
    rows, cols = tokens.shape
    block = gate_master.shape[1]
    half = rows * routes.shape[1] // nt
    every = 2 * nf * half
    pairs = nt // 2
    bf16 = jnp.bfloat16
    served = jax.ShapeDtypeStruct((1, block, nt * cols), bf16)
    hbm = pl.BlockSpec(memory_space=pl.ANY)
    vmem = pl.BlockSpec(memory_space=pltpu.VMEM)
    dma = pltpu.SemaphoreType.DMA
    return pl.pallas_call(
        functools.partial(kernel, nf, nt),
        out_shape=(served, served, served, jax.ShapeDtypeStruct((rows, cols), bf16)),
        in_specs=[vmem, vmem, hbm, hbm, hbm, vmem, vmem],
        out_specs=(hbm, hbm, hbm, vmem),
        scratch_shapes=[
            pltpu.VMEM((SLOTS, block, cols), jnp.float32),
            pltpu.VMEM((3, nt - 1, block, cols), bf16),
            pltpu.VMEM((3, nt, block, cols), bf16),
            pltpu.VMEM((nt * half, rows), bf16),
            pltpu.VMEM((nt * half, rows), bf16),
            pltpu.VMEM((nt, half, cols), bf16),
            pltpu.VMEM((nt, half, cols), bf16),
            pltpu.VMEM((nt, every, cols), bf16),
            pltpu.VMEM((every, block), jnp.float32),
            pltpu.VMEM((every, block), bf16),
            pltpu.VMEM((pairs, 2, every, cols), bf16),
            pltpu.VMEM((pairs, 2, every // 2, cols), bf16),
            pltpu.VMEM((pairs, nf, 2, half, cols), bf16),
            pltpu.VMEM((pairs, nf, 2, half, cols), bf16),
            pltpu.VMEM((nt * half, cols), bf16),
            dma((SLOTS,)),
            dma((3, nt - 1)), dma((3, nt - 1)),
            dma((nt - 1,)), dma((nt - 1,)),
            dma((nf,)), dma((nf,)),
            dma((nf,)), dma((nf,)),
            dma((pairs,)), dma((pairs,)),
            dma((pairs, nf)), dma((pairs, nf)),
            dma((nt - 1,)), dma((nt - 1,)),
            dma((3, nt)),
        ],
        compiler_params=pltpu.CompilerParams(
            collective_id=0, has_side_effects=True, vmem_limit_bytes=41 * 1024 * 1024
        ),
    )(tokens, norm_gain.reshape(1, cols), gate_master, up_master, down_master, routes.T, route_logits.T)


def solution(mesh):
    placed = (
        P("fs", "tp"),
        P("tp"),
        P(None, "fs", "tp"),
        P(None, "fs", "tp"),
        P(None, "fs", "tp"),
        P("fs", None),
        P("fs", None),
    )
    return jax.shard_map(
        local,
        mesh=mesh,
        in_specs=placed,
        out_specs=(P("tp", "fs", None), P("tp", "fs", None), P("tp", "fs", None), P("fs", "tp")),
        check_vma=False,
    )
```

profile of v0, /device:TPU:0, one launch (start us, length us, event | category | flops | bytes accessed | tf_op | source)
XLA Modules:
  0.0 156.1 jit_solution(1760734740764267413)
XLA Ops:
  0.6 0.0 copy-start
  0.6 0.9 copy-done
  1.5 0.0 copy-start.1
  1.5 0.7 copy-done.1
  2.2 0.0 copy-start.2
  2.2 0.7 copy-done.2
  2.9 0.0 copy-start.3
  2.9 0.7 copy-done.3
  3.6 146.4 %shard_map.102 = (bf16[1,896,2048]{2,1,0:T(8,128)(2,1)S(1)}, bf16[1,896,2048]{2,1,0:T(8,128)(2,1)S(1)}, bf16[1,896,2048]{2,1,0:T(8,128)(2,1)S(1)}, bf16[256,256]{1,0:T(8,128)(2,1)S(1)}) custom-call(bf16[256,256]{1,0:T(8,128)(2,1)S(1)} %copy-done, f32[1,256]{1,0:T(1,128)S(1)} %bitcast.5, f32[8,896,256]{2,1,0:T(8,128)} %gate_ref.1, f32[8,896,256]{2,1,0:T(8,128)} %up_ref.1, ...), custom_call_target="tpu_custom_call" | custom-call | tf_op jit(solution)/shard_map/pallas_call | solution.py:350
  149.9 1.8 %copy.15 = bf16[1,896,2048]{2,1,0:T(8,128)(2,1)} copy(bf16[1,896,2048]{2,1,0:T(8,128)(2,1)S(1)} %get-tuple-element.8) | data formatting | bytes 7340032
  151.8 1.8 %copy.16 = bf16[1,896,2048]{2,1,0:T(8,128)(2,1)} copy(bf16[1,896,2048]{2,1,0:T(8,128)(2,1)S(1)} %get-tuple-element.9) | data formatting | bytes 7340032
  153.6 1.8 %copy.17 = bf16[1,896,2048]{2,1,0:T(8,128)(2,1)} copy(bf16[1,896,2048]{2,1,0:T(8,128)(2,1)S(1)} %get-tuple-element.10) | data formatting | bytes 7340032
  155.5 0.7 copy.18
Async XLA Ops:
  0.6 0.9 copy-start
  1.5 0.7 copy-start.1
  2.2 0.7 copy-start.2
  2.9 0.7 copy-start.3
where the time goes:
time: 156 us
  Pallas kernels  146 us (94%)
  local copies, waits for them, and re-layouts  9.1 us (6%)
    pallas_call x1, Pallas kernels, local(): pl.pallas_call(functools.partial(kernel, nf, nt), out_shape=(served, serv...  146 us
    unnamed x12, local copies, waits for them, and re-layouts  9.1 us

commit v1 on v0

v1 whole, which is shorter than its diff:
```python
import functools

import jax
import jax.numpy as jnp
from jax import lax
from jax.experimental import pallas as pl
from jax.experimental.pallas import tpu as pltpu
from jax.sharding import PartitionSpec as P

epsilon = 1e-05
MESH = pl.DeviceIdType.MESH
NT = (((1,), (1,)), ((), ()))
NN = (((1,), (0,)), ((), ()))
TN = (((0,), (0,)), ((), ()))
SLOTS = 4
EARLY = 1


def dot(a, b, dims):
    return lax.dot_general(a, b, dims, preferred_element_type=jnp.float32)


def flipped(index, mask):
    result, bit = index, 1
    while bit <= mask:
        if mask & bit:
            result = result + bit * (1 - 2 * ((index // bit) % 2))
        bit *= 2
    return result


def kernel(
    nf, nt, tok_hbm, gain_hbm, gate_ref, up_ref, down_ref, routes_hbm, logits_hbm,
    wgu, wd, ret, comb_hi, comb_lo,
    tok, gain_ref, routes_ref, logits_ref, stage, snd, sdn, pick, xin, xall, gate_pre, hid,
    ship, pin, psum, zin, fin,
    in_sem, stage_sem, w_send, w_recv, d_send, d_recv, x_send, x_recv, z_send, z_recv, p_send, p_recv,
    h_send, h_recv, s_send, s_recv, r_send, r_recv,
):
    f, me = lax.axis_index("fs"), lax.axis_index("tp")
    parity = me % 2
    partner = me + 1 - 2 * parity
    rows, cols = tok.shape
    block = gate_ref.shape[1]
    parts, cc = wd.shape[1], wd.shape[3]
    half = pick.shape[1]
    cap = 2 * half
    experts = nt // 2
    pairs = nt // 2
    masters = (gate_ref, up_ref, down_ref)
    corner = [c for c in range(pairs - 1, 0, -1) if c.bit_count() > 1]
    near = [1] if pairs > 1 else []
    later = [c for c in range(pairs - 1, 1, -1) if c not in corner]

    def both(chips):
        return [k for c in chips for k in (2 * c + 1, 2 * c)]

    order = both(corner + near + later) + [1, 0]
    last = both(near + later) + [1, 0] + both(corner)
    jobs = [(w, k) for w in range(2) for k in order] + [(2, k) for k in last]

    def load(i):
        w, k = jobs[i]
        return pltpu.make_async_copy(
            masters[w].at[flipped(me, k)], stage.at[i % SLOTS], stage_sem.at[i % SLOTS]
        )

    def remote(src, dst, send, recv, to_f, to_t):
        return pltpu.make_async_remote_copy(
            src_ref=src, dst_ref=dst, send_sem=send, recv_sem=recv,
            device_id=(to_f, to_t), device_id_type=MESH,
        )

    small = [
        pltpu.make_async_copy(a, b, in_sem.at[i])
        for i, (a, b) in enumerate(
            ((gain_hbm, gain_ref), (routes_hbm, routes_ref), (logits_hbm, logits_ref), (tok_hbm, tok))
        )
    ]
    load(0).start()
    for copy in small:
        copy.start()
    for i in range(1, SLOTS):
        load(i).start()
    barrier = pltpu.get_barrier_semaphore()
    for k in range(1, nt):
        pl.semaphore_signal(barrier, inc=1, device_id=(f, flipped(me, k)), device_id_type=MESH)

    @pl.loop(1, nf)
    def _(d):
        pl.semaphore_signal(barrier, inc=1, device_id=((f + d) % nf, me), device_id_type=MESH)

    step = 128 if block % 128 == 0 else block

    def weight_copy(w, k):
        return remote(
            snd.at[w, k - 1], wgu.at[w, me], w_send.at[w, k - 1], w_recv.at[w, k - 1], f, flipped(me, k)
        )

    def down_copy(k, p):
        return remote(
            sdn.at[k - 1, p], wd.at[me, p], d_send.at[k - 1, p], d_recv.at[k - 1, p], f, flipped(me, k)
        )

    def convert(i):
        w, k = jobs[i]
        slot = i % SLOTS
        load(i).wait()
        gain = gain_ref[...]

        @pl.loop(0, block // step)
        def _(c):
            at = pl.ds(pl.multiple_of(c * step, 16), step)
            value = stage[slot, at, :]
            if w < 2:
                value = (value * gain).astype(jnp.bfloat16)
                if k:
                    snd[w, k - 1, at, :] = value
                else:
                    wgu[w, me, at, :] = value
            else:
                value = value.astype(jnp.bfloat16)
                for p in range(parts):
                    piece = value[:, p * cc : (p + 1) * cc]
                    if k:
                        sdn[k - 1, p, at, :] = piece
                    else:
                        wd[me, p, at, :] = piece

        if i + SLOTS < len(jobs):
            load(i + SLOTS).start()

    def send(i):
        w, k = jobs[i]
        if not k or k // 2 in later:
            return
        if w < 2:
            weight_copy(w, k).start()
        elif k % 2 == 0:
            for p in range(parts):
                down_copy(k + 1, p).start()
                down_copy(k, p).start()
        elif k == 1:
            for p in range(parts):
                down_copy(k, p).start()

    def x_copy(k):
        to = flipped(me, k)
        return remote(pick.at[to], xin.at[me], x_send.at[k - 1], x_recv.at[k - 1], f, to)

    def route():
        for copy in small[1:]:
            copy.wait()
        r0, r1 = routes_ref[0:1, :], routes_ref[1:2, :]
        l0, l1 = logits_ref[0:1, :], logits_ref[1:2, :]
        p0 = 1.0 / (1.0 + jnp.exp(l1 - l0))
        p1 = 1.0 / (1.0 + jnp.exp(l0 - l1))
        padded = -(-experts // 8) * 8
        ids = lax.broadcasted_iota(jnp.int32, (padded, rows), 0)
        first = jnp.where(ids == r0, 1.0, 0.0)
        second = jnp.where(ids == r1, 1.0, 0.0)
        chosen = first + second
        weight = first * p0 + second * p1
        before = lax.broadcasted_iota(jnp.int32, (rows, rows), 0)
        after = lax.broadcasted_iota(jnp.int32, (rows, rows), 1)
        upto = jnp.where(before <= after, 1.0, 0.0).astype(jnp.bfloat16)
        position = dot(chosen.astype(jnp.bfloat16), upto, NN) - 1.0
        slots = lax.broadcasted_iota(jnp.int32, (cap, rows), 0).astype(jnp.float32)
        for e in range(experts):
            hit = jnp.where(slots == position[e : e + 1, :], 1.0, 0.0) * chosen[e : e + 1, :]
            placed = hit.astype(jnp.bfloat16)
            scaled = hit * weight[e : e + 1, :]
            high = scaled.astype(jnp.bfloat16)
            at = pl.ds(e * cap, cap)
            comb_hi[at, :] = high
            comb_lo[at, :] = (scaled - high.astype(jnp.float32)).astype(jnp.bfloat16)
            got = dot(placed, tok[...], NN).astype(jnp.bfloat16)
            pick[2 * e] = got[:half]
            pick[2 * e + 1] = got[half:]
        xin[me] = pick[me]
        for k in order[:-1]:
            x_copy(k).start()

    small[0].wait()
    for i in range(EARLY):
        convert(i)
    pl.semaphore_wait(barrier, nt - 1 + nf - 1)
    for i in range(EARLY):
        send(i)
    route()
    for i in range(EARLY, len(jobs)):
        convert(i)
        send(i)

    def release(w):
        for k in both(corner):
            weight_copy(w, k).wait_send()
        for k in both(later):
            weight_copy(w, k).start()

    release(0)

    for k in order[:-1]:
        x_copy(k).wait_recv()
    total = jnp.zeros((half, 1), jnp.float32)
    for s in range(nt):
        v = xin[s].astype(jnp.float32)
        total = total + jnp.sum(v * v, axis=-1, keepdims=True)
    scale = lax.rsqrt(total / (nt * cols) + epsilon)

    def rows_of(p, g):
        return pl.ds(pl.multiple_of((2 * g + p) * half, 16), half)

    mine = rows_of(parity, f)
    for s in range(nt):
        xall[s, mine, :] = (xin[s].astype(jnp.float32) * scale).astype(jnp.bfloat16)

    def z_copy(d):
        here = xall.at[:, mine, :]
        return remote(here, here, z_send.at[d], z_recv.at[d], (f + d) % nf, me)

    def p_copy(d):
        here = xall.at[:, rows_of(parity, (f + nf - d) % nf), :]
        return remote(here, here, p_send.at[d], p_recv.at[d], f, partner)

    p_copy(0).start()

    @pl.loop(1, nf)
    def _(d):
        z_copy(d).start()

    @pl.loop(1, nf)
    def _(d):
        here = xall.at[:, rows_of(parity, (f + nf - d) % nf), :]
        remote(here, here, z_send.at[d], z_recv.at[d], (f + d) % nf, me).wait_recv()
        p_copy(d).start()

    @pl.loop(0, nf)
    def _(d):
        here = xall.at[:, rows_of(1 - parity, (f + nf - d) % nf), :]
        remote(here, here, p_send.at[d], p_recv.at[d], f, partner).wait_recv()

    def arrived(w, k):
        if k:
            s = flipped(me, k)
            remote(
                snd.at[w, k - 1], wgu.at[w, s], w_send.at[w, k - 1], w_recv.at[w, k - 1], f, s
            ).wait_recv()

    def product(w, at):
        acc = dot(xall[0], wgu[w, 0, at, :], NT)
        for s in range(1, nt):
            acc = acc + dot(xall[s], wgu[w, s, at, :], NT)
        return acc

    def tile(c):
        return pl.ds(pl.multiple_of(c * step, 16), step)

    def lanes(c):
        return pl.ds(pl.multiple_of(c * step, 128), step) if block % 128 == 0 else slice(None)

    for k in order:
        arrived(0, k)

    @pl.loop(0, block // step)
    def _(c):
        gate_pre[:, lanes(c)] = product(0, tile(c))

    release(1)
    for c in later:
        for p in range(parts):
            down_copy(2 * c + 1, p).start()
            down_copy(2 * c, p).start()
    for k in order:
        arrived(1, k)

    @pl.loop(0, block // step)
    def _(c):
        gate = gate_pre[:, lanes(c)]
        hid[:, lanes(c)] = (gate / (1.0 + jnp.exp(-gate)) * product(1, tile(c))).astype(jnp.bfloat16)

    groups = [(0, p) for p in range(parts)]
    groups += [(c, p) for p in range(parts) for c in near + later]
    groups += [(c, p) for p in range(parts) for c in corner]

    def took(k, p):
        s = flipped(me, k)
        if k:
            remote(
                sdn.at[k - 1, p], wd.at[s, p], d_send.at[k - 1, p], d_recv.at[k - 1, p], f, s
            ).wait_recv()
        return dot(hid[...], wd[s, p], NN)

    def h_copy(c, p):
        return remote(ship.at[c, p], pin.at[c, p], h_send.at[c, p], h_recv.at[c, p], f, partner)

    def s_copy(c, p, d):
        to = (f + d) % nf
        return remote(psum.at[c, p, to], zin.at[c, p, d], s_send.at[c, p, d], s_recv.at[c, p, d], to, me)

    def r_copy(c, p):
        return remote(
            fin.at[c, p], ret.at[p, pl.ds(pl.multiple_of((me // 2) * cap, 16), cap), :],
            r_send.at[c, p], r_recv.at[c, p], f, flipped(me, 2 * c),
        )

    def stage_a(c, p):
        ship[c, p] = took(2 * c + 1, p).astype(jnp.bfloat16)
        h_copy(c, p).start()

    def stage_b(c, p):
        own = took(2 * c, p)
        h_copy(c, p).wait_recv()
        total = (own + pin[c, p].astype(jnp.float32)).astype(jnp.bfloat16)
        for j in range(nf):
            psum[c, p, j] = total[j * cap : (j + 1) * cap]

        @pl.loop(1, nf)
        def _(d):
            s_copy(c, p, d).start()

    def stage_c(c, p):
        @pl.loop(1, nf)
        def _(d):
            s_copy(c, p, d).wait_recv()

        acc = psum[c, p, f].astype(jnp.float32)
        for d in range(1, nf):
            acc = acc + zin[c, p, d].astype(jnp.float32)
        if c:
            fin[c, p] = acc.astype(jnp.bfloat16)
            r_copy(c, p).start()
        else:
            ret[p, pl.ds(pl.multiple_of((me // 2) * cap, 16), cap), :] = acc.astype(jnp.bfloat16)

    for g, (c, p) in enumerate(groups):
        stage_a(c, p)
        stage_b(c, p)
        if g:
            stage_c(*groups[g - 1])
    stage_c(*groups[-1])

    for c in range(pairs):
        for p in range(parts):
            h_copy(c, p).wait_send()

            @pl.loop(1, nf)
            def _(d):
                s_copy(c, p, d).wait_send()

            if c:
                r_copy(c, p).wait_send()
    for k in range(1, nt):
        x_copy(k).wait_send()
        for w in range(2):
            if k // 2 not in corner:
                weight_copy(w, k).wait_send()
        for p in range(parts):
            down_copy(k, p).wait_send()
    p_copy(0).wait_send()

    @pl.loop(1, nf)
    def _(d):
        z_copy(d).wait_send()
        p_copy(d).wait_send()

    for c in range(1, pairs):
        for p in range(parts):
            r_copy(c, p).wait_recv()


def finish(wgu, wd, ret, comb_hi, comb_lo, gate_out, up_out, down_out, mixed_out, mixed, out_sem, mixed_sem):
    nt, parts, _, cc = wd.shape
    cols = parts * cc
    copies = []
    for s in range(nt):
        for w, out in enumerate((gate_out, up_out)):
            to = out.at[0, :, pl.ds(s * cols, cols)]
            copies.append(pltpu.make_async_copy(wgu.at[w, s], to, out_sem.at[w, s, 0]))
        for p in range(parts):
            to = down_out.at[0, :, pl.ds(s * cols + p * cc, cc)]
            copies.append(pltpu.make_async_copy(wd.at[s, p], to, out_sem.at[2, s, p]))
    for copy in copies:
        copy.start()
    for p in range(parts):
        back = ret[p]
        value = dot(comb_hi[...], back, TN) + dot(comb_lo[...], back, TN)
        mixed[:, p * cc : (p + 1) * cc] = value.astype(jnp.bfloat16)
    last = pltpu.make_async_copy(mixed, mixed_out, mixed_sem)
    last.start()
    for copy in copies:
        copy.wait()
    last.wait()


def local(tokens, norm_gain, gate_master, up_master, down_master, routes, route_logits):
    nf, nt = lax.axis_size("fs"), lax.axis_size("tp")
    rows, cols = tokens.shape
    block = gate_master.shape[1]
    half = rows * routes.shape[1] // nt
    cap = 2 * half
    every = nf * cap
    pairs = nt // 2
    parts = cols // 128 if cols % 128 == 0 else 1
    cc = cols // parts
    bf16 = jnp.bfloat16
    hbm = pl.BlockSpec(memory_space=pltpu.HBM)
    vmem = pl.BlockSpec(memory_space=pltpu.VMEM)
    dma = pltpu.SemaphoreType.DMA
    kept = (
        jax.ShapeDtypeStruct((2, nt, block, cols), bf16),
        jax.ShapeDtypeStruct((nt, parts, block, cc), bf16),
        jax.ShapeDtypeStruct((parts, nt * half, cc), bf16),
        jax.ShapeDtypeStruct((nt * half, rows), bf16),
        jax.ShapeDtypeStruct((nt * half, rows), bf16),
    )
    held = pl.pallas_call(
        functools.partial(kernel, nf, nt),
        out_shape=kept,
        in_specs=[hbm] * 7,
        out_specs=(vmem,) * 5,
        scratch_shapes=[
            pltpu.VMEM((rows, cols), bf16),
            pltpu.VMEM((1, cols), jnp.float32),
            pltpu.VMEM((2, rows), jnp.int32),
            pltpu.VMEM((2, rows), jnp.float32),
            pltpu.VMEM((SLOTS, block, cols), jnp.float32),
            pltpu.VMEM((2, nt - 1, block, cols), bf16),
            pltpu.VMEM((nt - 1, parts, block, cc), bf16),
            pltpu.VMEM((nt, half, cols), bf16),
            pltpu.VMEM((nt, half, cols), bf16),
            pltpu.VMEM((nt, every, cols), bf16),
            pltpu.VMEM((every, block), jnp.float32),
            pltpu.VMEM((every, block), bf16),
            pltpu.VMEM((pairs, parts, every, cc), bf16),
            pltpu.VMEM((pairs, parts, every, cc), bf16),
            pltpu.VMEM((pairs, parts, nf, cap, cc), bf16),
            pltpu.VMEM((pairs, parts, nf, cap, cc), bf16),
            pltpu.VMEM((pairs, parts, cap, cc), bf16),
            dma((4,)),
            dma((SLOTS,)),
            dma((2, nt - 1)), dma((2, nt - 1)),
            dma((nt - 1, parts)), dma((nt - 1, parts)),
            dma((nt - 1,)), dma((nt - 1,)),
            dma((nf,)), dma((nf,)),
            dma((nf,)), dma((nf,)),
            dma((pairs, parts)), dma((pairs, parts)),
            dma((pairs, parts, nf)), dma((pairs, parts, nf)),
            dma((pairs, parts)), dma((pairs, parts)),
        ],
        compiler_params=pltpu.CompilerParams(
            collective_id=0, has_side_effects=True, vmem_limit_bytes=40 * 1024 * 1024
        ),
    )(tokens, norm_gain.reshape(1, cols), gate_master, up_master, down_master, routes.T, route_logits.T)
    served = jax.ShapeDtypeStruct((1, block, nt * cols), bf16)
    return pl.pallas_call(
        finish,
        out_shape=(served, served, served, jax.ShapeDtypeStruct((rows, cols), bf16)),
        in_specs=[vmem] * 5,
        out_specs=(hbm,) * 4,
        scratch_shapes=[pltpu.VMEM((rows, cols), bf16), dma((3, nt, parts)), dma(())],
        compiler_params=pltpu.CompilerParams(vmem_limit_bytes=16 * 1024 * 1024),
    )(*held)


def solution(mesh):
    placed = (
        P("fs", "tp"),
        P("tp"),
        P(None, "fs", "tp"),
        P(None, "fs", "tp"),
        P(None, "fs", "tp"),
        P("fs", None),
        P("fs", None),
    )
    return jax.shard_map(
        local,
        mesh=mesh,
        in_specs=placed,
        out_specs=(P("tp", "fs", None), P("tp", "fs", None), P("tp", "fs", None), P("fs", "tp")),
        check_vma=False,
    )
```

time: 156 us -> 152 us (0.974)
  local copies, waits for them, and re-layouts: 9.1 us -> 2.94 us
  Pallas kernels: 146 us -> 148 us
    unnamed x12 -> x8, local copies, waits for them, and re-layouts: 9.1 us -> 2.94 us
    pallas_call x1 -> x2, Pallas kernels: 146 us -> 148 us  [the longest x1 143 us: local(): pl.pallas_call(functools.partial(kernel, nf, nt), out_shape=kept, in_spec...]
where the time goes in v1:
time: 152 us
  Pallas kernels  148 us (97%)
  local copies, waits for them, and re-layouts  2.94 us (2%)
    pallas_call x1, Pallas kernels, local(): pl.pallas_call(functools.partial(kernel, nf, nt), out_shape=kept, in_spec...  143 us
    pallas_call x1, Pallas kernels, local(): pl.pallas_call(finish, out_shape=(served, served, served, jax.ShapeDtypeS...  4.7 us

profile of v1, /device:TPU:0, one launch (start us, length us, event | category | flops | bytes accessed | tf_op | source)
XLA Modules:
  0.0 151.7 jit_solution(17285591048700794265)
XLA Ops:
  0.6 0.0 copy-start
  0.6 0.9 copy-done
  1.5 0.0 copy-start.1
  1.5 0.7 copy-done.1
  2.2 0.0 copy-start.2
  2.2 0.7 copy-done.2
  2.9 0.0 copy-start.3
  2.9 0.7 copy-done.3
  3.6 143.4 %shard_map.102 = (bf16[2,8,896,256]{3,2,1,0:T(8,128)(2,1)S(1)}, bf16[8,2,896,128]{3,2,1,0:T(8,128)(2,1)S(1)}, bf16[2,512,128]{2,1,0:T(8,128)(2,1)S(1)}, bf16[512,256]{1,0:T(8,128)(2,1)S(1)}, bf16[512,256]{1,0:T(8,128)(2,1)S(1)}) custom-call(bf16[256,256]{1,0:T(8,128)(2,1)S(1)} %copy-done, f32[1,256]{1,0:T(1,128)S(1)} %bitcast.5, f32[8,896,256]{2,1,0:T(8,128)} %gate_ref.1, ...), custom_call_target="tpu_custom_call" | custom-call | tf_op jit(solution)/shard_map/pallas_call | solution.py:417
  147.0 4.7 %shard_map.103 = (bf16[1,896,2048]{2,1,0:T(8,128)(2,1)}, bf16[1,896,2048]{2,1,0:T(8,128)(2,1)}, bf16[1,896,2048]{2,1,0:T(8,128)(2,1)}, bf16[256,256]{1,0:T(8,128)(2,1)}) custom-call(bf16[2,8,896,256]{3,2,1,0:T(8,128)(2,1)S(1)} %get-tuple-element.9.wgu, bf16[8,2,896,128]{3,2,1,0:T(8,128)(2,1)S(1)} %get-tuple-element.10.wd, ...), custom_call_target="tpu_custom_call" | custom-call | tf_op jit(solution)/shard_map/pallas_call | solution.py:456
Async XLA Ops:
  0.6 0.9 copy-start
  1.5 0.7 copy-start.1
  2.2 0.7 copy-start.2
  2.9 0.7 copy-start.3

commit v2 on v1

--- a/solution.py
+++ b/solution.py
@@ -13,7 +13,8 @@
 NN = (((1,), (0,)), ((), ()))
 TN = (((0,), (0,)), ((), ()))
 SLOTS = 4
-EARLY = 1
+EARLY = 2
+LAG = 2
 
 
 def dot(a, b, dims):
@@ -56,13 +57,27 @@
         return [k for c in chips for k in (2 * c + 1, 2 * c)]
 
     order = both(corner + near + later) + [1, 0]
+    even, odd = both(corner + near), both(near + corner)
+
+    def peer(k):
+        if isinstance(k, tuple):
+            a, b = k
+            return a + parity * (b - a), flipped(me, a) + parity * (flipped(me, b) - flipped(me, a))
+        return k, flipped(me, k)
+
+    crossing = list(zip(even, odd))
+    straight = both(later)
+    first = []
+    for j in range(max(len(crossing), len(straight))):
+        first += crossing[j : j + 1] + straight[j : j + 1]
+    first += [1, 0]
     last = both(near + later) + [1, 0] + both(corner)
-    jobs = [(w, k) for w in range(2) for k in order] + [(2, k) for k in last]
+    jobs = [(w, k) for w in range(2) for k in first] + [(2, k) for k in last]
 
     def load(i):
         w, k = jobs[i]
         return pltpu.make_async_copy(
-            masters[w].at[flipped(me, k)], stage.at[i % SLOTS], stage_sem.at[i % SLOTS]
+            masters[w].at[peer(k)[1]], stage.at[i % SLOTS], stage_sem.at[i % SLOTS]
         )
 
     def remote(src, dst, send, recv, to_f, to_t):
@@ -93,9 +108,8 @@
     step = 128 if block % 128 == 0 else block
 
     def weight_copy(w, k):
-        return remote(
-            snd.at[w, k - 1], wgu.at[w, me], w_send.at[w, k - 1], w_recv.at[w, k - 1], f, flipped(me, k)
-        )
+        k, to = peer(k)
+        return remote(snd.at[w, k - 1], wgu.at[w, me], w_send.at[w, k - 1], w_recv.at[w, k - 1], f, to)
 
     def down_copy(k, p):
         return remote(
@@ -115,7 +129,7 @@
             if w < 2:
                 value = (value * gain).astype(jnp.bfloat16)
                 if k:
-                    snd[w, k - 1, at, :] = value
+                    snd[w, peer(k)[0] - 1, at, :] = value
                 else:
                     wgu[w, me, at, :] = value
             else:
@@ -132,7 +146,7 @@
 
     def send(i):
         w, k = jobs[i]
-        if not k or k // 2 in later:
+        if not k:
             return
         if w < 2:
             weight_copy(w, k).start()
@@ -192,14 +206,6 @@
         convert(i)
         send(i)
 
-    def release(w):
-        for k in both(corner):
-            weight_copy(w, k).wait_send()
-        for k in both(later):
-            weight_copy(w, k).start()
-
-    release(0)
-
     for k in order[:-1]:
         x_copy(k).wait_recv()
     total = jnp.zeros((half, 1), jnp.float32)
@@ -266,11 +272,6 @@
     def _(c):
         gate_pre[:, lanes(c)] = product(0, tile(c))
 
-    release(1)
-    for c in later:
-        for p in range(parts):
-            down_copy(2 * c + 1, p).start()
-            down_copy(2 * c, p).start()
     for k in order:
         arrived(1, k)
 
@@ -336,9 +337,10 @@
     for g, (c, p) in enumerate(groups):
         stage_a(c, p)
         stage_b(c, p)
-        if g:
-            stage_c(*groups[g - 1])
-    stage_c(*groups[-1])
+        if g >= LAG:
+            stage_c(*groups[g - LAG])
+    for c, p in groups[-LAG:]:
+        stage_c(c, p)
 
     for c in range(pairs):
         for p in range(parts):
@@ -353,8 +355,7 @@
     for k in range(1, nt):
         x_copy(k).wait_send()
         for w in range(2):
-            if k // 2 not in corner:
-                weight_copy(w, k).wait_send()
+            weight_copy(w, k).wait_send()
         for p in range(parts):
             down_copy(k, p).wait_send()
     p_copy(0).wait_send()
@@ -414,6 +415,11 @@
         jax.ShapeDtypeStruct((nt * half, rows), bf16),
         jax.ShapeDtypeStruct((nt * half, rows), bf16),
     )
+    small = (
+        pltpu.with_memory_space_constraint(v, pltpu.HBM)
+        for v in (tokens, norm_gain.reshape(1, cols), routes.T, route_logits.T)
+    )
+    tokens, norm_gain, routes, route_logits = small
     held = pl.pallas_call(
         functools.partial(kernel, nf, nt),
         out_shape=kept,
@@ -451,7 +457,7 @@
         compiler_params=pltpu.CompilerParams(
             collective_id=0, has_side_effects=True, vmem_limit_bytes=40 * 1024 * 1024
         ),
-    )(tokens, norm_gain.reshape(1, cols), gate_master, up_master, down_master, routes.T, route_logits.T)
+    )(tokens, norm_gain, gate_master, up_master, down_master, routes, route_logits)
     served = jax.ShapeDtypeStruct((1, block, nt * cols), bf16)
     return pl.pallas_call(
         finish,

time: 152 us -> 145 us (0.954)
  Pallas kernels: 148 us -> 144 us
  local copies, waits for them, and re-layouts: 2.94 us -> 0 us
    pallas_call x1, Pallas kernels: 143 us -> 139 us  [local(): pl.pallas_call(functools.partial(kernel, nf, nt), out_shape=kept, in_spec...]
    unnamed x8 -> x0, local copies, waits for them, and re-layouts: 2.94 us -> none
where the time goes in v2:
time: 145 us
  Pallas kernels  144 us (99%)
    pallas_call x1, Pallas kernels, local(): pl.pallas_call(functools.partial(kernel, nf, nt), out_shape=kept, in_spec...  139 us
    pallas_call x1, Pallas kernels, local(): pl.pallas_call(finish, out_shape=(served, served, served, jax.ShapeDtypeS...  4.7 us

profile of v2, /device:TPU:0, one launch (start us, length us, event | category | flops | bytes accessed | tf_op | source)
XLA Modules:
  0.0 144.5 jit_solution(13241035349488908361)
XLA Ops:
  0.6 139.2 %shard_map.102 = (bf16[2,8,896,256]{3,2,1,0:T(8,128)(2,1)S(1)}, bf16[8,2,896,128]{3,2,1,0:T(8,128)(2,1)S(1)}, bf16[2,512,128]{2,1,0:T(8,128)(2,1)S(1)}, bf16[512,256]{1,0:T(8,128)(2,1)S(1)}, bf16[512,256]{1,0:T(8,128)(2,1)S(1)}) custom-call(bf16[256,256]{1,0:T(8,128)(2,1)} %tok_hbm.1, f32[1,256]{1,0:T(1,128)} %bitcast.5, f32[8,896,256]{2,1,0:T(8,128)} %gate_ref.1, ...), custom_call_target="tpu_custom_call" | custom-call | tf_op jit(solution)/shard_map/pallas_call | solution.py:423
  139.8 4.7 %shard_map.103 = (bf16[1,896,2048]{2,1,0:T(8,128)(2,1)}, bf16[1,896,2048]{2,1,0:T(8,128)(2,1)}, bf16[1,896,2048]{2,1,0:T(8,128)(2,1)}, bf16[256,256]{1,0:T(8,128)(2,1)}) custom-call(bf16[2,8,896,256]{3,2,1,0:T(8,128)(2,1)S(1)} %get-tuple-element.9.wgu, bf16[8,2,896,128]{3,2,1,0:T(8,128)(2,1)S(1)} %get-tuple-element.10.wd, ...), custom_call_target="tpu_custom_call" | custom-call | tf_op jit(solution)/shard_map/pallas_call | solution.py:462

commit v3 on v2

--- a/solution.py
+++ b/solution.py
@@ -1,4 +1,5 @@
 import functools
+import math
 
 import jax
 import jax.numpy as jnp
@@ -13,8 +14,10 @@
 NN = (((1,), (0,)), ((), ()))
 TN = (((0,), (0,)), ((), ()))
 SLOTS = 4
-EARLY = 2
+EARLY = 1
+ROUTED = 2
 LAG = 2
+SPARE = 8 * 1024 * 1024
 
 
 def dot(a, b, dims):
@@ -35,9 +38,10 @@
     wgu, wd, ret, comb_hi, comb_lo,
     tok, gain_ref, routes_ref, logits_ref, stage, snd, sdn, pick, xin, xall, gate_pre, hid,
     ship, pin, psum, zin, fin,
-    in_sem, stage_sem, w_send, w_recv, d_send, d_recv, x_send, x_recv, z_send, z_recv, p_send, p_recv,
-    h_send, h_recv, s_send, s_recv, r_send, r_recv,
+    in_sem, stage_sem, sent, w_recv, d_recv, one_recv, h_recv, s_recv,
 ):
+    w_send, d_send, x_send, z_send, p_send, h_send, s_send, r_send = (sent.at[i] for i in range(8))
+    x_recv, z_recv, p_recv, r_recv = (one_recv.at[i] for i in range(4))
     f, me = lax.axis_index("fs"), lax.axis_index("tp")
     parity = me % 2
     partner = me + 1 - 2 * parity
@@ -92,11 +96,12 @@
             ((gain_hbm, gain_ref), (routes_hbm, routes_ref), (logits_hbm, logits_ref), (tok_hbm, tok))
         )
     ]
-    load(0).start()
-    for copy in small:
-        copy.start()
-    for i in range(1, SLOTS):
+    small[0].start()
+    for i in range(SLOTS):
         load(i).start()
+        if not i:
+            for copy in small[1:]:
+                copy.start()
     barrier = pltpu.get_barrier_semaphore()
     for k in range(1, nt):
         pl.semaphore_signal(barrier, inc=1, device_id=(f, flipped(me, k)), device_id_type=MESH)
@@ -109,12 +114,10 @@
 
     def weight_copy(w, k):
         k, to = peer(k)
-        return remote(snd.at[w, k - 1], wgu.at[w, me], w_send.at[w, k - 1], w_recv.at[w, k - 1], f, to)
+        return remote(snd.at[w, k - 1], wgu.at[w, me], w_send, w_recv.at[w], f, to)
 
     def down_copy(k, p):
-        return remote(
-            sdn.at[k - 1, p], wd.at[me, p], d_send.at[k - 1, p], d_recv.at[k - 1, p], f, flipped(me, k)
-        )
+        return remote(sdn.at[k - 1, p], wd.at[me, p], d_send, d_recv.at[k - 1, p], f, flipped(me, k))
 
     def convert(i):
         w, k = jobs[i]
@@ -150,17 +153,17 @@
             return
         if w < 2:
             weight_copy(w, k).start()
-        elif k % 2 == 0:
-            for p in range(parts):
-                down_copy(k + 1, p).start()
-                down_copy(k, p).start()
         elif k == 1:
             for p in range(parts):
                 down_copy(k, p).start()
+        elif k % 2 == 0:
+            for p in range(parts):
+                down_copy(k, p).start()
+                down_copy(k + 1, p).start()
 
     def x_copy(k):
         to = flipped(me, k)
-        return remote(pick.at[to], xin.at[me], x_send.at[k - 1], x_recv.at[k - 1], f, to)
+        return remote(pick.at[to], xin.at[me], x_send, x_recv, f, to)
 
     def route():
         for copy in small[1:]:
@@ -201,13 +204,19 @@
     pl.semaphore_wait(barrier, nt - 1 + nf - 1)
     for i in range(EARLY):
         send(i)
-    route()
-    for i in range(EARLY, len(jobs)):
+    for i in range(EARLY, ROUTED):
         convert(i)
         send(i)
-
-    for k in order[:-1]:
-        x_copy(k).wait_recv()
+    route()
+    for i in range(ROUTED, len(jobs)):
+        convert(i)
+        send(i)
+
+    def whole(ref, send, recv):
+        return remote(ref, ref, send, recv, f, partner)
+
+    others = pl.ds(0, nt - 1)
+    whole(xin.at[others], x_send, x_recv).wait_recv()
     total = jnp.zeros((half, 1), jnp.float32)
     for s in range(nt):
         v = xin[s].astype(jnp.float32)
@@ -223,11 +232,11 @@
 
     def z_copy(d):
         here = xall.at[:, mine, :]
-        return remote(here, here, z_send.at[d], z_recv.at[d], (f + d) % nf, me)
+        return remote(here, here, z_send, z_recv, (f + d) % nf, me)
 
     def p_copy(d):
         here = xall.at[:, rows_of(parity, (f + nf - d) % nf), :]
-        return remote(here, here, p_send.at[d], p_recv.at[d], f, partner)
+        return remote(here, here, p_send, p_recv, f, partner)
 
     p_copy(0).start()
 
@@ -235,23 +244,18 @@
     def _(d):
         z_copy(d).start()
 
+    sides = whole(xall.at[:, pl.ds(0, (nf - 1) * half), :], z_send, z_recv)
+    across = whole(xall.at[:, pl.ds(0, nf * half), :], p_send, p_recv)
+    sides.wait_recv()
+
     @pl.loop(1, nf)
     def _(d):
-        here = xall.at[:, rows_of(parity, (f + nf - d) % nf), :]
-        remote(here, here, z_send.at[d], z_recv.at[d], (f + d) % nf, me).wait_recv()
         p_copy(d).start()
 
-    @pl.loop(0, nf)
-    def _(d):
-        here = xall.at[:, rows_of(1 - parity, (f + nf - d) % nf), :]
-        remote(here, here, p_send.at[d], p_recv.at[d], f, partner).wait_recv()
-
-    def arrived(w, k):
-        if k:
-            s = flipped(me, k)
-            remote(
-                snd.at[w, k - 1], wgu.at[w, s], w_send.at[w, k - 1], w_recv.at[w, k - 1], f, s
-            ).wait_recv()
+    across.wait_recv()
+
+    def arrived(w):
+        whole(wgu.at[w, others], w_send, w_recv.at[w]).wait_recv()
 
     def product(w, at):
         acc = dot(xall[0], wgu[w, 0, at, :], NT)
@@ -265,15 +269,13 @@
     def lanes(c):
         return pl.ds(pl.multiple_of(c * step, 128), step) if block % 128 == 0 else slice(None)
 
-    for k in order:
-        arrived(0, k)
+    arrived(0)
 
     @pl.loop(0, block // step)
     def _(c):
         gate_pre[:, lanes(c)] = product(0, tile(c))
 
-    for k in order:
-        arrived(1, k)
+    arrived(1)
 
     @pl.loop(0, block // step)
     def _(c):
@@ -284,33 +286,32 @@
     groups += [(c, p) for p in range(parts) for c in near + later]
     groups += [(c, p) for p in range(parts) for c in corner]
 
+    up = f // ((nf + 1) // 2)
+
     def took(k, p):
         s = flipped(me, k)
         if k:
-            remote(
-                sdn.at[k - 1, p], wd.at[s, p], d_send.at[k - 1, p], d_recv.at[k - 1, p], f, s
-            ).wait_recv()
+            whole(wd.at[s, p], d_send, d_recv.at[k - 1, p]).wait_recv()
         return dot(hid[...], wd[s, p], NN)
 
     def h_copy(c, p):
-        return remote(ship.at[c, p], pin.at[c, p], h_send.at[c, p], h_recv.at[c, p], f, partner)
+        return remote(ship.at[c, p], pin.at[c, p], h_send, h_recv.at[c, p], f, partner)
 
     def s_copy(c, p, d):
+        d = up * d + (1 - up) * (nf - d)
         to = (f + d) % nf
-        return remote(psum.at[c, p, to], zin.at[c, p, d], s_send.at[c, p, d], s_recv.at[c, p, d], to, me)
+        return remote(psum.at[c, p, to], zin.at[c, p, d], s_send, s_recv.at[c, p], to, me)
 
     def r_copy(c, p):
-        return remote(
-            fin.at[c, p], ret.at[p, pl.ds(pl.multiple_of((me // 2) * cap, 16), cap), :],
-            r_send.at[c, p], r_recv.at[c, p], f, flipped(me, 2 * c),
-        )
+        there = ret.at[p, pl.ds(pl.multiple_of((me // 2) * cap, 16), cap), :]
+        return remote(fin.at[c, p], there, r_send, r_recv, f, flipped(me, 2 * c + 1))
 
     def stage_a(c, p):
-        ship[c, p] = took(2 * c + 1, p).astype(jnp.bfloat16)
+        ship[c, p] = took(2 * c, p).astype(jnp.bfloat16)
         h_copy(c, p).start()
 
     def stage_b(c, p):
-        own = took(2 * c, p)
+        own = took(2 * c + 1, p)
         h_copy(c, p).wait_recv()
         total = (own + pin[c, p].astype(jnp.float32)).astype(jnp.bfloat16)
         for j in range(nf):
@@ -321,18 +322,12 @@
             s_copy(c, p, d).start()
 
     def stage_c(c, p):
-        @pl.loop(1, nf)
-        def _(d):
-            s_copy(c, p, d).wait_recv()
-
+        whole(zin.at[c, p, pl.ds(1, nf - 1)], s_send, s_recv.at[c, p]).wait_recv()
         acc = psum[c, p, f].astype(jnp.float32)
         for d in range(1, nf):
             acc = acc + zin[c, p, d].astype(jnp.float32)
-        if c:
-            fin[c, p] = acc.astype(jnp.bfloat16)
-            r_copy(c, p).start()
-        else:
-            ret[p, pl.ds(pl.multiple_of((me // 2) * cap, 16), cap), :] = acc.astype(jnp.bfloat16)
+        fin[c, p] = acc.astype(jnp.bfloat16)
+        r_copy(c, p).start()
 
     for g, (c, p) in enumerate(groups):
         stage_a(c, p)
@@ -342,55 +337,35 @@
     for c, p in groups[-LAG:]:
         stage_c(c, p)
 
-    for c in range(pairs):
-        for p in range(parts):
-            h_copy(c, p).wait_send()
-
-            @pl.loop(1, nf)
-            def _(d):
-                s_copy(c, p, d).wait_send()
-
-            if c:
-                r_copy(c, p).wait_send()
-    for k in range(1, nt):
-        x_copy(k).wait_send()
-        for w in range(2):
-            weight_copy(w, k).wait_send()
-        for p in range(parts):
-            down_copy(k, p).wait_send()
-    p_copy(0).wait_send()
-
-    @pl.loop(1, nf)
-    def _(d):
-        z_copy(d).wait_send()
-        p_copy(d).wait_send()
-
-    for c in range(1, pairs):
-        for p in range(parts):
-            r_copy(c, p).wait_recv()
-
-
-def finish(wgu, wd, ret, comb_hi, comb_lo, gate_out, up_out, down_out, mixed_out, mixed, out_sem, mixed_sem):
+    whole(pick.at[others], x_send, x_recv).wait_send()
+    whole(snd, w_send, w_recv.at[0]).wait_send()
+    whole(sdn, d_send, d_recv.at[0, 0]).wait_send()
+    sides.wait_send()
+    across.wait_send()
+    whole(ship, h_send, h_recv.at[0, 0]).wait_send()
+    whole(psum.at[:, :, pl.ds(0, nf - 1)], s_send, s_recv.at[0, 0]).wait_send()
+    whole(fin, r_send, r_recv).wait_send()
+    whole(ret, r_send, r_recv).wait_recv()
+
+
+def finish(wgu, wd, ret, comb_hi, comb_lo, gate_out, up_out, down_out, mixed_out, mixed, out_sem):
     nt, parts, _, cc = wd.shape
     cols = parts * cc
-    copies = []
     for s in range(nt):
         for w, out in enumerate((gate_out, up_out)):
             to = out.at[0, :, pl.ds(s * cols, cols)]
-            copies.append(pltpu.make_async_copy(wgu.at[w, s], to, out_sem.at[w, s, 0]))
+            pltpu.make_async_copy(wgu.at[w, s], to, out_sem.at[w]).start()
         for p in range(parts):
             to = down_out.at[0, :, pl.ds(s * cols + p * cc, cc)]
-            copies.append(pltpu.make_async_copy(wd.at[s, p], to, out_sem.at[2, s, p]))
-    for copy in copies:
-        copy.start()
+            pltpu.make_async_copy(wd.at[s, p], to, out_sem.at[2]).start()
     for p in range(parts):
         back = ret[p]
         value = dot(comb_hi[...], back, TN) + dot(comb_lo[...], back, TN)
         mixed[:, p * cc : (p + 1) * cc] = value.astype(jnp.bfloat16)
-    last = pltpu.make_async_copy(mixed, mixed_out, mixed_sem)
+    last = pltpu.make_async_copy(mixed, mixed_out, out_sem.at[3])
     last.start()
-    for copy in copies:
-        copy.wait()
+    for w, out in enumerate((gate_out, up_out, down_out)):
+        pltpu.make_async_copy(out, out, out_sem.at[w]).wait()
     last.wait()
 
 
@@ -415,56 +390,57 @@
         jax.ShapeDtypeStruct((nt * half, rows), bf16),
         jax.ShapeDtypeStruct((nt * half, rows), bf16),
     )
-    small = (
-        pltpu.with_memory_space_constraint(v, pltpu.HBM)
-        for v in (tokens, norm_gain.reshape(1, cols), routes.T, route_logits.T)
+    operands = (
+        tokens, norm_gain.reshape(1, cols), gate_master, up_master, down_master, routes.T, route_logits.T,
     )
-    tokens, norm_gain, routes, route_logits = small
+    operands = [pltpu.with_memory_space_constraint(v, pltpu.HBM) for v in operands]
+    buffers = [
+        pltpu.VMEM((rows, cols), bf16),
+        pltpu.VMEM((1, cols), jnp.float32),
+        pltpu.VMEM((2, rows), jnp.int32),
+        pltpu.VMEM((2, rows), jnp.float32),
+        pltpu.VMEM((SLOTS, block, cols), jnp.float32),
+        pltpu.VMEM((2, nt - 1, block, cols), bf16),
+        pltpu.VMEM((nt - 1, parts, block, cc), bf16),
+        pltpu.VMEM((nt, half, cols), bf16),
+        pltpu.VMEM((nt, half, cols), bf16),
+        pltpu.VMEM((nt, every, cols), bf16),
+        pltpu.VMEM((every, block), jnp.float32),
+        pltpu.VMEM((every, block), bf16),
+        pltpu.VMEM((pairs, parts, every, cc), bf16),
+        pltpu.VMEM((pairs, parts, every, cc), bf16),
+        pltpu.VMEM((pairs, parts, nf, cap, cc), bf16),
+        pltpu.VMEM((pairs, parts, nf, cap, cc), bf16),
+        pltpu.VMEM((pairs, parts, cap, cc), bf16),
+    ]
+    grant = sum(math.prod(v.shape) * jnp.dtype(v.dtype).itemsize for v in buffers) + SPARE
     held = pl.pallas_call(
         functools.partial(kernel, nf, nt),
         out_shape=kept,
         in_specs=[hbm] * 7,
         out_specs=(vmem,) * 5,
         scratch_shapes=[
-            pltpu.VMEM((rows, cols), bf16),
-            pltpu.VMEM((1, cols), jnp.float32),
-            pltpu.VMEM((2, rows), jnp.int32),
-            pltpu.VMEM((2, rows), jnp.float32),
-            pltpu.VMEM((SLOTS, block, cols), jnp.float32),
-            pltpu.VMEM((2, nt - 1, block, cols), bf16),
-            pltpu.VMEM((nt - 1, parts, block, cc), bf16),
-            pltpu.VMEM((nt, half, cols), bf16),
-            pltpu.VMEM((nt, half, cols), bf16),
-            pltpu.VMEM((nt, every, cols), bf16),
-            pltpu.VMEM((every, block), jnp.float32),
-            pltpu.VMEM((every, block), bf16),
-            pltpu.VMEM((pairs, parts, every, cc), bf16),
-            pltpu.VMEM((pairs, parts, every, cc), bf16),
-            pltpu.VMEM((pairs, parts, nf, cap, cc), bf16),
-            pltpu.VMEM((pairs, parts, nf, cap, cc), bf16),
-            pltpu.VMEM((pairs, parts, cap, cc), bf16),
+            *buffers,
             dma((4,)),
             dma((SLOTS,)),
-            dma((2, nt - 1)), dma((2, nt - 1)),
-            dma((nt - 1, parts)), dma((nt - 1, parts)),
-            dma((nt - 1,)), dma((nt - 1,)),
-            dma((nf,)), dma((nf,)),
-            dma((nf,)), dma((nf,)),
-            dma((pairs, parts)), dma((pairs, parts)),
-            dma((pairs, parts, nf)), dma((pairs, parts, nf)),
-            dma((pairs, parts)), dma((pairs, parts)),
+            dma((8,)),
+            dma((2,)),
+            dma((nt - 1, parts)),
+            dma((4,)),
+            dma((pairs, parts)),
+            dma((pairs, parts)),
         ],
         compiler_params=pltpu.CompilerParams(
-            collective_id=0, has_side_effects=True, vmem_limit_bytes=40 * 1024 * 1024
+            collective_id=0, has_side_effects=True, vmem_limit_bytes=grant
         ),
-    )(tokens, norm_gain, gate_master, up_master, down_master, routes, route_logits)
+    )(*operands)
     served = jax.ShapeDtypeStruct((1, block, nt * cols), bf16)
     return pl.pallas_call(
         finish,
         out_shape=(served, served, served, jax.ShapeDtypeStruct((rows, cols), bf16)),
         in_specs=[vmem] * 5,
         out_specs=(hbm,) * 4,
-        scratch_shapes=[pltpu.VMEM((rows, cols), bf16), dma((3, nt, parts)), dma(())],
+        scratch_shapes=[pltpu.VMEM((rows, cols), bf16), dma((4,))],
         compiler_params=pltpu.CompilerParams(vmem_limit_bytes=16 * 1024 * 1024),
     )(*held)
 

time: 145 us -> 142 us (0.979)
  Pallas kernels: 144 us -> 141 us
    pallas_call x1, Pallas kernels: 139 us -> 137 us  [local(): pl.pallas_call(functools.partial(kernel, nf, nt), out_shape=kept, in_spec...]
where the time goes in v3:
time: 142 us
  Pallas kernels  141 us (99%)
    pallas_call x1, Pallas kernels, local(): pl.pallas_call(functools.partial(kernel, nf, nt), out_shape=kept, in_spec...  137 us
    pallas_call x1, Pallas kernels, local(): pl.pallas_call(finish, out_shape=(served, served, served, jax.ShapeDtypeS...  4.3 us

profile of v3, /device:TPU:0, one launch (start us, length us, event | category | flops | bytes accessed | tf_op | source)
XLA Modules:
  0.0 141.6 jit_solution(5885111241184286471)
XLA Ops:
  0.6 136.6 %shard_map.102 = (bf16[2,8,896,256]{3,2,1,0:T(8,128)(2,1)S(1)}, bf16[8,2,896,128]{3,2,1,0:T(8,128)(2,1)S(1)}, bf16[2,512,128]{2,1,0:T(8,128)(2,1)S(1)}, bf16[512,256]{1,0:T(8,128)(2,1)S(1)}, bf16[512,256]{1,0:T(8,128)(2,1)S(1)}) custom-call(bf16[256,256]{1,0:T(8,128)(2,1)} %tok_hbm.1, f32[1,256]{1,0:T(1,128)} %bitcast.5, f32[8,896,256]{2,1,0:T(8,128)} %gate_ref.1, ...), custom_call_target="tpu_custom_call" | custom-call | tf_op jit(solution)/shard_map/pallas_call | solution.py:417
  137.3 4.3 %shard_map.103 = (bf16[1,896,2048]{2,1,0:T(8,128)(2,1)}, bf16[1,896,2048]{2,1,0:T(8,128)(2,1)}, bf16[1,896,2048]{2,1,0:T(8,128)(2,1)}, bf16[256,256]{1,0:T(8,128)(2,1)}) custom-call(bf16[2,8,896,256]{3,2,1,0:T(8,128)(2,1)S(1)} %get-tuple-element.9.wgu, bf16[8,2,896,128]{3,2,1,0:T(8,128)(2,1)S(1)} %get-tuple-element.10.wd, ...), custom_call_target="tpu_custom_call" | custom-call | tf_op jit(solution)/shard_map/pallas_call | solution.py:438
